TPU v7x, 32 devices: a whole 2x2x4 slice. The times are simulated.
32 devices in a mesh: sp: 8 (over z, y), tp: 4 (over x, core).
Axes of the slice: x: 2, y: 2, z: 4, core: 2. Of those that a mesh axis runs over, the one named last changes fastest.
Arguments:
- residual_in: bfloat16 [3072, 2048], P(('sp', 'tp')), may hold values from -6 to 6
- queries: bfloat16 [3072, 2048], P('sp', 'tp'), may hold values from -180 to 180
- keys: bfloat16 [3072, 2048], P('sp', 'tp'), may hold values from -9 to 9
- values: bfloat16 [3072, 2048], P('sp', 'tp'), may hold values from -6 to 6
- mix_lambda: float32 [16], P('tp'), may hold values from 0.3 to 0.8
- head_gain: float32 [128], replicated, may hold values from 0.1 to 1.9
- out_weight: bfloat16 [2048, 2048], P('tp'), may hold values from -0.125 to 0.125
- norm_gain: float32 [2048], replicated, may hold values from 0.1 to 1.9
- gate_weight: bfloat16 [2048, 5632], P('sp', 'tp'), may hold values from -0.125 to 0.125
- up_weight: bfloat16 [2048, 5632], P('sp', 'tp'), may hold values from -0.125 to 0.125
- down_weight: bfloat16 [5632, 2048], P('tp', 'sp'), may hold values from -0.078125 to 0.078125
Outputs:
- layer_out: bfloat16 [3072, 2048], P(('sp', 'tp'))
All inputs are finite; a program needn't handle non-finite values.
Results may differ from a plain program's by a relative error of at most 0.014.
Values may be sent and summed in bfloat16 or wider, within the bound.
A program may use at most 128 MiB of HBM per device.

v0:
```python
import math
import jax
import jax.numpy as jnp
from jax import lax
from jax.sharding import PartitionSpec as P

DH = 64
VD = 128


def body(
    residual_in,
    queries,
    keys,
    values,
    mix_lambda,
    head_gain,
    out_weight,
    norm_gain,
    gate_weight,
    up_weight,
    down_weight,
):
    tp_count = lax.axis_size("tp")
    tok_local = queries.shape[0]
    heads_local = mix_lambda.shape[0]
    rows_local = tok_local // tp_count
    query_four = queries.reshape(tok_local, heads_local, 2, DH)
    inverse_root = 1.0 / math.sqrt(DH)

    def one_block(state, block):
        top, total, weighted = state
        key_block, value_block = block
        scores = (
            jnp.einsum("qhcd,khcd->hcqk", query_four, key_block, preferred_element_type=jnp.float32)
            * inverse_root
        )
        new_top = jnp.maximum(top, jnp.max(scores, axis=-1))
        rescale = jnp.exp(top - new_top)
        expo = jnp.exp(scores - new_top[..., None])
        total = total * rescale + jnp.sum(expo, axis=-1)
        weighted = weighted * rescale[..., None] + jnp.einsum(
            "hcqk,khe->hcqe",
            expo.astype(jnp.bfloat16),
            value_block,
            preferred_element_type=jnp.float32,
        )
        return ((new_top, total, weighted), None)

    start_state = (
        jnp.full((heads_local, 2, tok_local), -1e30, jnp.float32),
        jnp.zeros((heads_local, 2, tok_local), jnp.float32),
        jnp.zeros((heads_local, 2, tok_local, VD), jnp.float32),
    )
    key_piece = lax.all_gather(keys, "sp", axis=0, tiled=True)
    value_piece = lax.all_gather(values, "sp", axis=0, tiled=True)
    count = key_piece.shape[0]
    shards = max(count // tok_local, 1)
    unit = count // shards
    group = max(
        (g for g in range(1, shards + 1) if shards % g == 0 and g * unit <= max(1536, unit))
    )
    width = group * unit
    blocks = count // width
    key_blocks = key_piece.reshape(blocks, width, heads_local, 2, DH)
    value_blocks = value_piece.reshape(blocks, width, heads_local, VD)
    state, unused = lax.scan(one_block, start_state, (key_blocks, value_blocks))
    top, total, weighted = state
    maps = weighted / total[..., None]
    mixed = maps[:, 0] - mix_lambda[:, None, None] * maps[:, 1]
    head_scale = lax.rsqrt(jnp.mean(mixed * mixed, axis=-1, keepdims=True) + 1e-06)
    head_out = (mixed * head_scale * head_gain).astype(jnp.bfloat16)
    attended = jnp.transpose(head_out, (1, 0, 2)).reshape(tok_local, heads_local * VD)
    summed = lax.psum(
        jnp.dot(attended, out_weight, preferred_element_type=jnp.float32).astype(jnp.bfloat16), "tp"
    ).astype(jnp.float32)
    residual_all = lax.all_gather(residual_in, "tp", axis=0, tiled=True)
    after_all = residual_all.astype(jnp.float32) + summed
    row_scale = lax.rsqrt(jnp.mean(after_all * after_all, axis=-1, keepdims=True) + 1e-06)
    all_rows = (after_all * row_scale * norm_gain).astype(jnp.bfloat16)
    after_mix = lax.dynamic_slice_in_dim(
        after_all, lax.axis_index("tp") * rows_local, rows_local, 0
    )
    gate_all, up_all, down_all = (
        lax.all_gather(gate_weight, "sp", axis=0, tiled=True),
        lax.all_gather(up_weight, "sp", axis=0, tiled=True),
        lax.all_gather(down_weight, "sp", axis=1, tiled=True),
    )
    gate = jnp.dot(all_rows, gate_all, preferred_element_type=jnp.float32)
    up = jnp.dot(all_rows, up_all, preferred_element_type=jnp.float32)
    hidden = (jax.nn.silu(gate) * up).astype(jnp.bfloat16)
    mixer = lax.psum_scatter(
        jnp.dot(hidden, down_all, preferred_element_type=jnp.float32).astype(jnp.bfloat16),
        "tp",
        scatter_dimension=0,
        tiled=True,
    ).astype(jnp.float32)
    return (after_mix + 0.5 * mixer).astype(jnp.bfloat16)


def solution(mesh):
    return jax.shard_map(
        body,
        mesh=mesh,
        in_specs=(
            P(("sp", "tp"), None),
            P("sp", "tp"),
            P("sp", "tp"),
            P("sp", "tp"),
            P("tp"),
            P(),
            P("tp", None),
            P(),
            P("sp", "tp"),
            P("sp", "tp"),
            P("tp", "sp"),
        ),
        out_specs=P(("sp", "tp"), None),
        check_vma=False,
    )
```

profile of v0, /device:TPU:0, one launch (start us, length us, event | category | flops | bytes accessed | tf_op | source)
XLA Modules:
  0.0 579.6 jit_solution(15325134770839630398)
XLA Ops:
  6.5 0.7 all-gather.9.cloned.1.call-update
  7.3 0.0 all-gather.11.cloned.1.call-start
  7.3 0.7 all-gather.11.cloned.1.call-update
  8.0 0.0 all-gather.7.cloned.1.call-start
  8.1 0.7 all-gather.7.cloned.1.call-update
  8.7 0.0 all-reduce.2.cloned.1.call-start
  8.8 1.2 copy.17
  10.0 62.3 %all-gather.9.cloned.1.call-done = bf16[3072,512]{1,0:T(8,128)(2,1)} async-done(((bf16[384,512]{1,0:T(8,128)(2,1)}), bf16[3072,512]{1,0:T(8,128)(2,1)}) %all-gather.9.cloned.1.call-update) | async-done | bytes 3145744 | tf_op jit(solution)/shard_map/all_gather | solution.py:55
  72.3 12.5 %reshape.39 = bf16[2,1536,4,2,64]{4,3,2,1,0:T(2,128)(2,1)} reshape(bf16[3072,512]{1,0:T(8,128)(2,1)} %all-gather.9.cloned.1.call-done) | data formatting | bytes 6291456 | tf_op jit(solution)/shard_map/reshape | solution.py:65
  84.8 15.4 %copy.18 = bf16[2,1536,4,2,64]{1,4,3,2,0:T(8,128)(2,1)} copy(bf16[2,1536,4,2,64]{4,3,2,1,0:T(2,128)(2,1)} %reshape.39) | data formatting | bytes 6291456
  100.2 33.0 %all-gather.11.cloned.1.call-done = bf16[3072,512]{1,0:T(8,128)(2,1)} async-done(((bf16[384,512]{1,0:T(8,128)(2,1)}), bf16[3072,512]{1,0:T(8,128)(2,1)}) %all-gather.11.cloned.1.call-update) | async-done | bytes 3145744 | tf_op jit(solution)/shard_map/all_gather | solution.py:56
  133.2 5.6 reshape.36
  138.7 63.8 %while.15 = (s32[]{:T(128)}, f32[4,2,384]{2,1,0:T(2,128)S(1)}, f32[4,2,384]{2,1,0:T(2,128)S(1)}, f32[4,2,384,128]{3,2,1,0:T(8,128)}, bf16[2,1536,4,2,64]{1,4,3,2...) while((s32[]{:T(128)}, f32[4,2,384]{2,1,0:T(2,128)S(1)}, ...), condition=%wide.region_3.4_spmd.clone, body=%wide.region_0.3_spmd.clone.sunk | while | flops 1850883072 | bytes 79233688 | solution.py:67
  138.7 10.6 %bitcast_reduce_fusion.2 = (f32[4,2,384]{2,1,0:T(2,128)S(1)}, f32[4,2,1536,384]{3,2,1,0:T(8,128)}) fusion(bf16[384,4,2,64]{0,3,2,1:T(8,128)(2,1)S(1)} %get-tuple-element.170, bf16[2,1536,4,2,64]{1,4,3,2,0:T(8,128)(2,1)} %get-tuple-element.169, s32[]{:T(128)} %get-tuple-element.156), kind=kOutput, calls=%fused_computation.1.clone.1 | convolution fusion | flops 613413888 | bytes 20853248 | tf_op jit(solution)/shard_map/while/body/eval_jaxpr/qhcd,khcd->hcqk/dot_general | solution.py:35
  149.4 9.5 %fusion.37 = f32[4,2,384]{2,1,0:T(2,128)S(1)} fusion(f32[4,2,1536,384]{3,2,1,0:T(8,128)} %get-tuple-element.144, f32[4,2,384]{2,1,0:T(2,128)S(1)} %fusion.36), kind=kLoop, calls=%fused_computation.4.clone.1 | loop fusion | flops 14152704 | bytes 18898944 | tf_op jit(solution)/shard_map/while/body/eval_jaxpr/reduce_sum | solution.py:41
  158.9 1.8 constant_dynamic-slice_fusion.2
  160.7 8.8 %fusion.39 = f32[4,2,384,128]{3,2,1,0:T(8,128)S(1)} fusion(f32[4,2,384,128]{3,2,1,0:T(8,128)S(1)} %copy-done.1, bf16[1,1536,4,128]{3,2,1,0:T(4,128)(2,1)S(1)} %constant_dynamic-slice_fusion.2, f32[4,2,1536,384]{3,2,1,0:T(8,128)} %get-tuple-element.144, f32[4,2,384]{2,1,0:T(2,128)S(1)} %fusion.36, f32[4,2,384]{2,1,0:T(2,128)S(1)} %get-tuple-element.146, ...), kind=kOutput, calls=%fused_computation.12.clone.1 | convolution fusion | flops 1223294976 | bytes 23617536 | tf_op jit(solution)/shard_map/while/body/eval_jaxpr/hcqk,khe->hcqe/dot_general | solution.py:42
  169.5 1.1 copy-done.2
  170.7 10.5 %bitcast_reduce_fusion.2 = (f32[4,2,384]{2,1,0:T(2,128)S(1)}, f32[4,2,1536,384]{3,2,1,0:T(8,128)}) fusion(bf16[384,4,2,64]{0,3,2,1:T(8,128)(2,1)S(1)} %get-tuple-element.170, bf16[2,1536,4,2,64]{1,4,3,2,0:T(8,128)(2,1)} %get-tuple-element.169, s32[]{:T(128)} %get-tuple-element.156), kind=kOutput, calls=%fused_computation.1.clone.1 | convolution fusion | flops 613413888 | bytes 20853248 | tf_op jit(solution)/shard_map/while/body/eval_jaxpr/qhcd,khcd->hcqk/dot_general | solution.py:35
  181.2 9.4 %fusion.37 = f32[4,2,384]{2,1,0:T(2,128)S(1)} fusion(f32[4,2,1536,384]{3,2,1,0:T(8,128)} %get-tuple-element.144, f32[4,2,384]{2,1,0:T(2,128)S(1)} %fusion.36), kind=kLoop, calls=%fused_computation.4.clone.1 | loop fusion | flops 14152704 | bytes 18898944 | tf_op jit(solution)/shard_map/while/body/eval_jaxpr/reduce_sum | solution.py:41
  190.7 1.8 constant_dynamic-slice_fusion.2
  192.6 8.8 %fusion.39 = f32[4,2,384,128]{3,2,1,0:T(8,128)S(1)} fusion(f32[4,2,384,128]{3,2,1,0:T(8,128)S(1)} %copy-done.1, bf16[1,1536,4,128]{3,2,1,0:T(4,128)(2,1)S(1)} %constant_dynamic-slice_fusion.2, f32[4,2,1536,384]{3,2,1,0:T(8,128)} %get-tuple-element.144, f32[4,2,384]{2,1,0:T(2,128)S(1)} %fusion.36, f32[4,2,384]{2,1,0:T(2,128)S(1)} %get-tuple-element.146, ...), kind=kOutput, calls=%fused_computation.12.clone.1 | convolution fusion | flops 1223294976 | bytes 23617536 | tf_op jit(solution)/shard_map/while/body/eval_jaxpr/hcqk,khe->hcqe/dot_general | solution.py:42
  201.4 1.1 copy-done.2
  202.5 3.1 copy.21
  205.6 1.5 broadcast_divide_fusion
  207.1 0.2 multiply_reduce_fusion.1
  207.3 0.2 multiply_convert_fusion.1
  207.6 2.2 convolution_convert_fusion.1
  209.7 0.0 all-reduce.2.cloned.1.call-update
  209.8 0.0 all-gather.13.cloned.1.call-start
  209.8 0.5 all-gather.13.cloned.1.call-update
  210.4 0.0 all-gather.15.cloned.1.call-start
  210.4 0.5 all-gather.15.cloned.1.call-update
  210.9 0.0 all-gather.17.cloned.1.call-start
  211.0 0.7 all-gather.17.cloned.1.call-update
  211.7 0.0 copy-start.5
  211.7 0.0 reduce-scatter.2.cloned.1.call-start
  211.7 0.0 all-gather.7.cloned.1.call-done
  211.8 39.7 %all-reduce.2.cloned.1.call-done = bf16[384,2048]{1,0:T(8,128)(2,1)} async-done(((bf16[384,2048]{1,0:T(8,128)(2,1)}), bf16[384,2048]{1,0:T(8,128)(2,1)}) %all-reduce.2.cloned.1.call-update) | async-done | bytes 1572880 | tf_op jit(solution)/shard_map/psum | solution.py:74
  251.5 4.0 convert_add_fusion
  255.5 90.4 %all-gather.13.cloned.1.call-done = bf16[2048,1408]{1,0:T(8,128)(2,1)} async-done(((bf16[256,1408]{1,0:T(8,128)(2,1)}), bf16[2048,1408]{1,0:T(8,128)(2,1)}) %all-gather.13.cloned.1.call-update) | async-done | bytes 5767184 | tf_op jit(solution)/shard_map/all_gather | solution.py:85
  345.9 7.6 %fusion.21 = f32[384,1408]{1,0:T(8,128)} fusion(bf16[2048,1408]{1,0:T(8,128)(2,1)} %all-gather.13.cloned.1.call-done, f32[2048]{0:T(1024)S(1)} %copy-done.5, f32[384]{0:T(512)S(1)} %add_rsqrt_fusion.1, bf16[384,2048]{1,0:T(8,128)(2,1)} %all-reduce.2.cloned.1.call-done, bf16[384,2048]{1,0:T(8,128)(2,1)} %all-gather.7.cloned.1.call-done), kind=kOutput, calls=%fused_computation.40 | convolution fusion | flops 2219311104 | bytes 11085312 | tf_op jit(solution)/shard_map/dot_general | solution.py:89
  353.5 85.0 %all-gather.15.cloned.1.call-done = bf16[2048,1408]{1,0:T(8,128)(2,1)} async-done(((bf16[256,1408]{1,0:T(8,128)(2,1)}), bf16[2048,1408]{1,0:T(8,128)(2,1)}) %all-gather.15.cloned.1.call-update) | async-done | bytes 5767184 | tf_op jit(solution)/shard_map/all_gather | solution.py:86
  438.5 93.4 %all-gather.17.cloned.1.call-done = bf16[1408,2048]{1,0:T(8,128)(2,1)} async-done(((bf16[1408,256]{1,0:T(8,128)(2,1)}), bf16[1408,2048]{1,0:T(8,128)(2,1)}) %all-gather.17.cloned.1.call-update) | async-done | bytes 5767184 | tf_op jit(solution)/shard_map/all_gather | solution.py:87
  531.9 12.4 %convolution_convert_fusion = bf16[384,2048]{1,0:T(8,128)(2,1)} fusion(bf16[1408,2048]{1,0:T(8,128)(2,1)} %all-gather.17.cloned.1.call-done, bf16[2048,1408]{1,0:T(8,128)(2,1)} %all-gather.15.cloned.1.call-done, f32[384,1408]{1,0:T(8,128)} %fusion.21, f32[2048]{0:T(1024)S(1)} %copy-done.5, f32[384]{0:T(512)S(1)} %add_rsqrt_fusion.1, ...), kind=kOutput, calls=%fused_computation.27 | convolution fusion | flops 4437934080 | bytes 18425344 | tf_op jit(solution)/shard_map/dot_general | solution.py:93
  544.3 0.0 reduce-scatter.2.cloned.1.call-update
  544.3 26.4 %reduce-scatter.2.cloned.1.call-done = bf16[96,2048]{1,0:T(8,128)(2,1)} async-done(((bf16[384,2048]{1,0:T(8,128)(2,1)}), bf16[96,2048]{1,0:T(8,128)(2,1)}) %reduce-scatter.2.cloned.1.call-update) | async-done | bytes 393232 | tf_op jit(solution)/shard_map/reduce_scatter | solution.py:92
  570.7 2.1 add_convert_fusion
  (26 shorter events, 0.2 us)
Async XLA Ops:
  6.5 201.0 %copy-start = (bf16[512,2048]{1,0:T(8,128)(2,1)S(1)}, bf16[512,2048]{1,0:T(8,128)(2,1)}, u32[]{:S(2)}) copy-start(bf16[512,2048]{1,0:T(8,128)(2,1)} %param.19) | copy-start | bytes 6291460
  6.5 65.8 %all-gather.9.cloned.1.call-start = ((), (), s32[]{:S(2)}) async-start(), calls=%async_computation.2 | async-start | bytes 3538944 | tf_op jit(solution)/shard_map/all_gather | solution.py:55
  7.3 125.9 %all-gather.11.cloned.1.call-start = ((), (), s32[]{:S(2)}) async-start(), calls=%async_computation.3 | async-start | bytes 3538944 | tf_op jit(solution)/shard_map/all_gather | solution.py:56
  8.0 203.8 %all-gather.7.cloned.1.call-start = ((), (), s32[]{:S(2)}) async-start(), calls=%async_computation.1 | async-start | bytes 1966080 | tf_op jit(solution)/shard_map/all_gather | solution.py:77
  8.7 242.7 %all-reduce.2.cloned.1.call-start = ((), (), s32[]{:S(2)}) async-start(), calls=%async_computation.4 | async-start | bytes 3145728 | tf_op jit(solution)/shard_map/psum | solution.py:74
  158.8 1.9 copy-start.1
  169.5 1.1 copy-start.2
  190.7 1.9 copy-start.1
  201.3 1.1 copy-start.2
  205.6 1.6 copy-start.3
  205.6 1.8 copy-start.4
  209.8 136.1 %all-gather.13.cloned.1.call-start = ((), (), s32[]{:S(2)}) async-start(), calls=%async_computation.5 | async-start | bytes 6488064 | tf_op jit(solution)/shard_map/all_gather | solution.py:85
  210.4 228.1 %all-gather.15.cloned.1.call-start = ((), (), s32[]{:S(2)}) async-start(), calls=%async_computation.6 | async-start | bytes 6488064 | tf_op jit(solution)/shard_map/all_gather | solution.py:86
  210.9 321.0 %all-gather.17.cloned.1.call-start = ((), (), s32[]{:S(2)}) async-start(), calls=%async_computation.7 | async-start | bytes 6488064 | tf_op jit(solution)/shard_map/all_gather | solution.py:87
  211.7 134.2 %copy-start.5 = (f32[2048]{0:T(1024)S(1)}, f32[2048]{0:T(1024)}, u32[]{:S(2)}) copy-start(f32[2048]{0:T(1024)} %param.20) | copy-start | bytes 24580
  211.7 359.0 %reduce-scatter.2.cloned.1.call-start = ((), (), s32[]{:S(2)}) async-start(), calls=%async_computation.8 | async-start | bytes 1966080 | tf_op jit(solution)/shard_map/reduce_scatter | solution.py:92
Sparse Core Ops, SparseCore 0:
  9.5 62.7 all-gather.8
  74.5 58.6 all-gather.10
  134.7 18.2 all-gather.6
  209.9 41.5 all-reduce.1
  253.5 92.3 all-gather.12
  347.9 90.5 all-gather.14
  440.5 91.2 all-gather.16
  544.4 26.2 reduce-scatter.1
where the time goes:
time: 581 us; the launch traced here: 580 us
  waiting for transfers between devices  434 us (75%)
  matrix products  60.9 us (10%)
  local copies, waits for them, and re-layouts  43.7 us (8%)
  other arithmetic  27.1 us (5%)
  between operations  13.6 us (2%)
    all_gather x1, waiting for transfers between devices, body(): lax.all_gather(down_weight, 'sp', axis=1, tiled=True)  93.4 us
    all_gather x1, waiting for transfers between devices, body(): lax.all_gather(gate_weight, 'sp', axis=0, tiled=True)  90.4 us
    all_gather x1, waiting for transfers between devices, body(): lax.all_gather(up_weight, 'sp', axis=0, tiled=True)  85 us
    all_gather x1, waiting for transfers between devices, body(): key_piece = lax.all_gather(keys, 'sp', axis=0, tiled=True)  62.3 us
    psum x1, waiting for transfers between devices, body(): lax.psum(jnp.dot(attended, out_weight, preferred_element_type=jnp.float32...  39.7 us
    all_gather x1, waiting for transfers between devices, body(): value_piece = lax.all_gather(values, 'sp', axis=0, tiled=True)  33 us
    reduce_scatter x1, waiting for transfers between devices, body(): lax.psum_scatter(jnp.dot(hidden, down_all, preferred_element_type=jnp.flo...  26.4 us
    dot_general x2, matrix products, one_block(): jnp.einsum('qhcd,khcd->hcqk', query_four, key_block, preferred_element_ty...  21.1 us
  transfers between devices with their start and end apart: 8, of which 7 were waited for; matrix products, arithmetic and copies ran while one was open for 20% of the time, Pallas kernels for 0%

commit v1 on v0

--- a/solution.py
+++ b/solution.py
@@ -71,8 +71,12 @@
     head_scale = lax.rsqrt(jnp.mean(mixed * mixed, axis=-1, keepdims=True) + 1e-06)
     head_out = (mixed * head_scale * head_gain).astype(jnp.bfloat16)
     attended = jnp.transpose(head_out, (1, 0, 2)).reshape(tok_local, heads_local * VD)
-    summed = lax.psum(
-        jnp.dot(attended, out_weight, preferred_element_type=jnp.float32).astype(jnp.bfloat16), "tp"
+    summed = jnp.sum(
+        lax.all_gather(
+            jnp.dot(attended, out_weight, preferred_element_type=jnp.float32).astype(jnp.bfloat16),
+            "tp",
+        ),
+        axis=0,
     ).astype(jnp.float32)
     residual_all = lax.all_gather(residual_in, "tp", axis=0, tiled=True)
     after_all = residual_all.astype(jnp.float32) + summed

time: 581 us -> 605 us (1.041)
  waiting for transfers between devices: 434 us -> 453 us
    all_gather x0 -> x1, waiting for transfers between devices: none -> 42.6 us  [body(): lax.all_gather(jnp.dot(attended, out_weight, preferred_element_type=jnp.f...]
    psum x1 -> x0, waiting for transfers between devices: 39.7 us -> none  [body(): lax.psum(jnp.dot(attended, out_weight, preferred_element_type=jnp.float32...]
    all_gather x1, waiting for transfers between devices: 0.02 us -> 15.4 us  [body(): residual_all = lax.all_gather(residual_in, 'tp', axis=0, tiled=True)]
  transfers between devices with their start and end apart: 8 -> 8, of which waited for: 7 -> 8; matrix products, arithmetic and copies ran while one was open for 20% -> 8% of each run, Pallas kernels for 0% -> 0%
where the time goes in v1:
time: 605 us; the launch traced here: 604 us
  waiting for transfers between devices  453 us (75%)
  matrix products  60.6 us (10%)
  local copies, waits for them, and re-layouts  43.8 us (7%)
  other arithmetic  32.8 us (5%)
  between operations  13.6 us (2%)
    all_gather x1, waiting for transfers between devices, body(): lax.all_gather(down_weight, 'sp', axis=1, tiled=True)  93.4 us
    all_gather x1, waiting for transfers between devices, body(): lax.all_gather(gate_weight, 'sp', axis=0, tiled=True)  90.3 us
    all_gather x1, waiting for transfers between devices, body(): lax.all_gather(up_weight, 'sp', axis=0, tiled=True)  85 us
    all_gather x1, waiting for transfers between devices, body(): key_piece = lax.all_gather(keys, 'sp', axis=0, tiled=True)  63 us
    all_gather x1, waiting for transfers between devices, body(): lax.all_gather(jnp.dot(attended, out_weight, preferred_element_type=jnp.f...  42.6 us
    all_gather x1, waiting for transfers between devices, body(): value_piece = lax.all_gather(values, 'sp', axis=0, tiled=True)  33 us
    reduce_scatter x1, waiting for transfers between devices, body(): lax.psum_scatter(jnp.dot(hidden, down_all, preferred_element_type=jnp.flo...  26.4 us
    dot_general x2, matrix products, one_block(): jnp.einsum('qhcd,khcd->hcqk', query_four, key_block, preferred_element_ty...  21.1 us
  transfers between devices with their start and end apart: 8, of which 8 were waited for; matrix products, arithmetic and copies ran while one was open for 8% of the time, Pallas kernels for 0%

profile of v1, /device:TPU:0, one launch (start us, length us, event | category | flops | bytes accessed | tf_op | source)
XLA Modules:
  0.0 603.9 jit_solution(17917128461578991965)
XLA Ops:
  6.5 0.7 all-gather.11.cloned.1.call-update
  7.3 0.0 all-gather.13.cloned.1.call-start
  7.3 0.7 all-gather.13.cloned.1.call-update
  8.0 0.0 all-gather.21.cloned.1.call-start
  8.1 1.2 copy.17
  9.3 63.0 %all-gather.11.cloned.1.call-done = bf16[3072,512]{1,0:T(8,128)(2,1)} async-done(((bf16[384,512]{1,0:T(8,128)(2,1)}), bf16[3072,512]{1,0:T(8,128)(2,1)}) %all-gather.11.cloned.1.call-update) | async-done | bytes 3145744 | tf_op jit(solution)/shard_map/all_gather | solution.py:55
  72.3 12.5 %reshape.40 = bf16[2,1536,4,2,64]{4,3,2,1,0:T(2,128)(2,1)} reshape(bf16[3072,512]{1,0:T(8,128)(2,1)} %all-gather.11.cloned.1.call-done) | data formatting | bytes 6291456 | tf_op jit(solution)/shard_map/reshape | solution.py:65
  84.8 15.4 %copy.18 = bf16[2,1536,4,2,64]{1,4,3,2,0:T(8,128)(2,1)} copy(bf16[2,1536,4,2,64]{4,3,2,1,0:T(2,128)(2,1)} %reshape.40) | data formatting | bytes 6291456
  100.2 33.0 %all-gather.13.cloned.1.call-done = bf16[3072,512]{1,0:T(8,128)(2,1)} async-done(((bf16[384,512]{1,0:T(8,128)(2,1)}), bf16[3072,512]{1,0:T(8,128)(2,1)}) %all-gather.13.cloned.1.call-update) | async-done | bytes 3145744 | tf_op jit(solution)/shard_map/all_gather | solution.py:56
  133.2 5.6 reshape.36
  138.7 63.7 %while.15 = (s32[]{:T(128)}, f32[4,2,384]{2,1,0:T(2,128)S(1)}, f32[4,2,384]{2,1,0:T(2,128)S(1)}, f32[4,2,384,128]{3,2,1,0:T(8,128)}, bf16[2,1536,4,2,64]{1,4,3,2...) while((s32[]{:T(128)}, f32[4,2,384]{2,1,0:T(2,128)S(1)}, ...), condition=%wide.region_3.4_spmd.clone, body=%wide.region_0.3_spmd.clone.sunk | while | flops 1850883072 | bytes 79233688 | solution.py:67
  138.7 10.5 %bitcast_reduce_fusion.2 = (f32[4,2,384]{2,1,0:T(2,128)S(1)}, f32[4,2,1536,384]{3,2,1,0:T(8,128)}) fusion(bf16[384,4,2,64]{0,3,2,1:T(8,128)(2,1)S(1)} %get-tuple-element.170, bf16[2,1536,4,2,64]{1,4,3,2,0:T(8,128)(2,1)} %get-tuple-element.169, s32[]{:T(128)} %get-tuple-element.156), kind=kOutput, calls=%fused_computation.1.clone.1 | convolution fusion | flops 613413888 | bytes 20853248 | tf_op jit(solution)/shard_map/while/body/eval_jaxpr/qhcd,khcd->hcqk/dot_general | solution.py:35
  149.3 9.4 %fusion.37 = f32[4,2,384]{2,1,0:T(2,128)S(1)} fusion(f32[4,2,1536,384]{3,2,1,0:T(8,128)} %get-tuple-element.144, f32[4,2,384]{2,1,0:T(2,128)S(1)} %fusion.36), kind=kLoop, calls=%fused_computation.4.clone.1 | loop fusion | flops 14152704 | bytes 18898944 | tf_op jit(solution)/shard_map/while/body/eval_jaxpr/reduce_sum | solution.py:41
  158.8 1.8 constant_dynamic-slice_fusion.2
  160.6 8.8 %fusion.39 = f32[4,2,384,128]{3,2,1,0:T(8,128)S(1)} fusion(f32[4,2,384,128]{3,2,1,0:T(8,128)S(1)} %copy-done.1, bf16[1,1536,4,128]{3,2,1,0:T(4,128)(2,1)S(1)} %constant_dynamic-slice_fusion.2, f32[4,2,1536,384]{3,2,1,0:T(8,128)} %get-tuple-element.144, f32[4,2,384]{2,1,0:T(2,128)S(1)} %fusion.36, f32[4,2,384]{2,1,0:T(2,128)S(1)} %get-tuple-element.146, ...), kind=kOutput, calls=%fused_computation.12.clone.1 | convolution fusion | flops 1223294976 | bytes 23617536 | tf_op jit(solution)/shard_map/while/body/eval_jaxpr/hcqk,khe->hcqe/dot_general | solution.py:42
  169.4 1.2 copy-done.2
  170.6 10.5 %bitcast_reduce_fusion.2 = (f32[4,2,384]{2,1,0:T(2,128)S(1)}, f32[4,2,1536,384]{3,2,1,0:T(8,128)}) fusion(bf16[384,4,2,64]{0,3,2,1:T(8,128)(2,1)S(1)} %get-tuple-element.170, bf16[2,1536,4,2,64]{1,4,3,2,0:T(8,128)(2,1)} %get-tuple-element.169, s32[]{:T(128)} %get-tuple-element.156), kind=kOutput, calls=%fused_computation.1.clone.1 | convolution fusion | flops 613413888 | bytes 20853248 | tf_op jit(solution)/shard_map/while/body/eval_jaxpr/qhcd,khcd->hcqk/dot_general | solution.py:35
  181.2 9.4 %fusion.37 = f32[4,2,384]{2,1,0:T(2,128)S(1)} fusion(f32[4,2,1536,384]{3,2,1,0:T(8,128)} %get-tuple-element.144, f32[4,2,384]{2,1,0:T(2,128)S(1)} %fusion.36), kind=kLoop, calls=%fused_computation.4.clone.1 | loop fusion | flops 14152704 | bytes 18898944 | tf_op jit(solution)/shard_map/while/body/eval_jaxpr/reduce_sum | solution.py:41
  190.6 1.8 constant_dynamic-slice_fusion.2
  192.5 8.8 %fusion.39 = f32[4,2,384,128]{3,2,1,0:T(8,128)S(1)} fusion(f32[4,2,384,128]{3,2,1,0:T(8,128)S(1)} %copy-done.1, bf16[1,1536,4,128]{3,2,1,0:T(4,128)(2,1)S(1)} %constant_dynamic-slice_fusion.2, f32[4,2,1536,384]{3,2,1,0:T(8,128)} %get-tuple-element.144, f32[4,2,384]{2,1,0:T(2,128)S(1)} %fusion.36, f32[4,2,384]{2,1,0:T(2,128)S(1)} %get-tuple-element.146, ...), kind=kOutput, calls=%fused_computation.12.clone.1 | convolution fusion | flops 1223294976 | bytes 23617536 | tf_op jit(solution)/shard_map/while/body/eval_jaxpr/hcqk,khe->hcqe/dot_general | solution.py:42
  201.3 1.2 copy-done.2
  202.5 3.1 copy.21
  205.6 1.5 broadcast_divide_fusion
  207.1 0.2 multiply_reduce_fusion.1
  207.3 0.2 multiply_convert_fusion.1
  207.5 2.2 convolution_convert_fusion.1
  209.8 0.0 all-gather.21.cloned.1.call-update
  209.8 0.0 all-gather.9.cloned.1.call-start
  209.8 0.5 all-gather.9.cloned.1.call-update
  210.4 0.0 all-gather.15.cloned.1.call-start
  210.4 0.5 all-gather.15.cloned.1.call-update
  211.0 0.0 all-gather.17.cloned.1.call-start
  211.0 0.5 all-gather.17.cloned.1.call-update
  211.5 0.0 all-gather.19.cloned.1.call-start
  211.6 0.7 all-gather.19.cloned.1.call-update
  212.3 0.0 reduce-scatter.2.cloned.1.call-start
  212.3 42.6 %all-gather.21.cloned.1.call-done = bf16[1536,2048]{1,0:T(8,128)(2,1)} async-done(((bf16[384,2048]{1,0:T(8,128)(2,1)}), bf16[1536,2048]{1,0:T(8,128)(2,1)}) %all-gather.21.cloned.1.call-update) | async-done | bytes 6291472 | tf_op jit(solution)/shard_map/all_gather | solution.py:75
  255.0 5.7 reduce_sum.40
  260.7 15.4 %all-gather.9.cloned.1.call-done = bf16[384,2048]{1,0:T(8,128)(2,1)} async-done(((bf16[96,2048]{1,0:T(8,128)(2,1)}), bf16[384,2048]{1,0:T(8,128)(2,1)}) %all-gather.9.cloned.1.call-update) | async-done | bytes 1572880 | tf_op jit(solution)/shard_map/all_gather | solution.py:81
  276.0 4.0 convert_add_fusion
  280.1 90.3 %all-gather.15.cloned.1.call-done = bf16[2048,1408]{1,0:T(8,128)(2,1)} async-done(((bf16[256,1408]{1,0:T(8,128)(2,1)}), bf16[2048,1408]{1,0:T(8,128)(2,1)}) %all-gather.15.cloned.1.call-update) | async-done | bytes 5767184 | tf_op jit(solution)/shard_map/all_gather | solution.py:89
  370.4 7.6 %fusion.21 = f32[384,1408]{1,0:T(8,128)} fusion(bf16[2048,1408]{1,0:T(8,128)(2,1)} %all-gather.15.cloned.1.call-done, f32[2048]{0:T(1024)S(1)} %copy-done.5, f32[384]{0:T(512)S(1)} %add_rsqrt_fusion.1, bf16[384,2048]{1,0:T(8,128)(2,1)} %reduce_sum.40, bf16[384,2048]{1,0:T(8,128)(2,1)} %all-gather.9.cloned.1.call-done), kind=kOutput, calls=%fused_computation.40 | convolution fusion | flops 2219311104 | bytes 11085312 | tf_op jit(solution)/shard_map/dot_general | solution.py:93
  378.1 85.0 %all-gather.17.cloned.1.call-done = bf16[2048,1408]{1,0:T(8,128)(2,1)} async-done(((bf16[256,1408]{1,0:T(8,128)(2,1)}), bf16[2048,1408]{1,0:T(8,128)(2,1)}) %all-gather.17.cloned.1.call-update) | async-done | bytes 5767184 | tf_op jit(solution)/shard_map/all_gather | solution.py:90
  463.0 93.4 %all-gather.19.cloned.1.call-done = bf16[1408,2048]{1,0:T(8,128)(2,1)} async-done(((bf16[1408,256]{1,0:T(8,128)(2,1)}), bf16[1408,2048]{1,0:T(8,128)(2,1)}) %all-gather.19.cloned.1.call-update) | async-done | bytes 5767184 | tf_op jit(solution)/shard_map/all_gather | solution.py:91
  556.4 12.2 %convolution_convert_fusion = bf16[384,2048]{1,0:T(8,128)(2,1)} fusion(bf16[1408,2048]{1,0:T(8,128)(2,1)} %all-gather.19.cloned.1.call-done, bf16[2048,1408]{1,0:T(8,128)(2,1)} %all-gather.17.cloned.1.call-done, f32[384,1408]{1,0:T(8,128)} %fusion.21, f32[2048]{0:T(1024)S(1)} %copy-done.5, f32[384]{0:T(512)S(1)} %add_rsqrt_fusion.1, ...), kind=kOutput, calls=%fused_computation.27 | convolution fusion | flops 4437934080 | bytes 18425344 | tf_op jit(solution)/shard_map/dot_general | solution.py:97
  568.6 0.0 reduce-scatter.2.cloned.1.call-update
  568.6 26.4 %reduce-scatter.2.cloned.1.call-done = bf16[96,2048]{1,0:T(8,128)(2,1)} async-done(((bf16[384,2048]{1,0:T(8,128)(2,1)}), bf16[96,2048]{1,0:T(8,128)(2,1)}) %reduce-scatter.2.cloned.1.call-update) | async-done | bytes 393232 | tf_op jit(solution)/shard_map/reduce_scatter | solution.py:96
  595.0 2.1 add_convert_fusion
  (27 shorter events, 0.2 us)
Async XLA Ops:
  6.5 201.0 %copy-start = (bf16[512,2048]{1,0:T(8,128)(2,1)S(1)}, bf16[512,2048]{1,0:T(8,128)(2,1)}, u32[]{:S(2)}) copy-start(bf16[512,2048]{1,0:T(8,128)(2,1)} %param.19) | copy-start | bytes 6291460
  6.5 65.8 %all-gather.11.cloned.1.call-start = ((), (), s32[]{:S(2)}) async-start(), calls=%async_computation.2 | async-start | bytes 3538944 | tf_op jit(solution)/shard_map/all_gather | solution.py:55
  7.3 125.9 %all-gather.13.cloned.1.call-start = ((), (), s32[]{:S(2)}) async-start(), calls=%async_computation.3 | async-start | bytes 3538944 | tf_op jit(solution)/shard_map/all_gather | solution.py:56
  8.0 247.0 %all-gather.21.cloned.1.call-start = ((), (), s32[]{:S(2)}) async-start(), calls=%async_computation.8 | async-start | bytes 7864320 | tf_op jit(solution)/shard_map/all_gather | solution.py:75
  158.7 1.9 copy-start.1
  169.4 1.2 copy-start.2
  190.6 1.9 copy-start.1
  201.3 1.2 copy-start.2
  205.5 1.6 copy-start.3
  205.5 1.8 copy-start.4
  209.8 66.3 %all-gather.9.cloned.1.call-start = ((), (), s32[]{:S(2)}) async-start(), calls=%async_computation.1 | async-start | bytes 1966080 | tf_op jit(solution)/shard_map/all_gather | solution.py:81
  210.4 160.1 %all-gather.15.cloned.1.call-start = ((), (), s32[]{:S(2)}) async-start(), calls=%async_computation.4 | async-start | bytes 6488064 | tf_op jit(solution)/shard_map/all_gather | solution.py:89
  211.0 252.1 %all-gather.17.cloned.1.call-start = ((), (), s32[]{:S(2)}) async-start(), calls=%async_computation.5 | async-start | bytes 6488064 | tf_op jit(solution)/shard_map/all_gather | solution.py:90
  211.5 344.9 %all-gather.19.cloned.1.call-start = ((), (), s32[]{:S(2)}) async-start(), calls=%async_computation.6 | async-start | bytes 6488064 | tf_op jit(solution)/shard_map/all_gather | solution.py:91
  212.3 382.7 %reduce-scatter.2.cloned.1.call-start = ((), (), s32[]{:S(2)}) async-start(), calls=%async_computation.7 | async-start | bytes 1966080 | tf_op jit(solution)/shard_map/reduce_scatter | solution.py:96
  260.7 109.7 %copy-start.5 = (f32[2048]{0:T(1024)S(1)}, f32[2048]{0:T(1024)}, u32[]{:S(2)}) copy-start(f32[2048]{0:T(1024)} %param.20) | copy-start | bytes 24580
Sparse Core Ops, SparseCore 0:
  9.5 62.7 all-gather.10
  74.5 58.6 all-gather.12
  209.9 45.0 all-gather.20
  256.4 19.6 all-gather.8
  278.1 92.3 all-gather.14
  372.5 90.5 all-gather.16
  465.1 91.2 all-gather.18
  568.7 26.2 reduce-scatter.1
